TPU v7x, 32 devices: a whole 2x2x4 slice. The times are simulated.
32 devices in a mesh: fs: 8 (over z, core), tp: 4 (over y, x).
Axes of the slice: x: 2, y: 2, z: 4, core: 2. Of those that a mesh axis runs over, the one named last changes fastest.
Arguments:
- gate_pre: bfloat16 [8192, 5632], P('fs', 'tp'), may hold values from -6 to 6
- up_pre: bfloat16 [8192, 5632], P('fs', 'tp'), may hold values from -6 to 6
- gate_taps: bfloat16 [3, 5632], replicated, may hold values from -3.5 to 3.5
- up_taps: bfloat16 [3, 5632], replicated, may hold values from -3.5 to 3.5
- down_proj: bfloat16 [5632, 2048], P('tp', 'fs'), may hold values from -0.078125 to 0.078125
- cotangent: bfloat16 [8192, 2048], P(('fs', 'tp')), may hold values from -6 to 6
Outputs:
- gate_grad: bfloat16 [8192, 5632], P('fs', 'tp')
- up_grad: bfloat16 [8192, 5632], P('fs', 'tp')
- down_grad: float32 [5632, 2048], P('tp', 'fs')
- row_norms: float32 [5632], P('tp')
- tap_grads: float32 [2, 3, 5632], replicated
All inputs are finite; a program needn't handle non-finite values.
Results may differ from a plain program's by a relative error of at most 0.0042.
Values may be sent and summed in bfloat16 or wider, within the bound.
A program may use at most 128 MiB of HBM per device.

v0:
```python
import math

import jax
import jax.numpy as jnp
from jax import lax
from jax.sharding import PartitionSpec as P


def from_behind(block, axis, distance):
    devices = range(lax.axis_size(axis))
    route = [(i - distance, i) for i in devices if i - distance in devices]
    return lax.ppermute(block, axis, route)


def body(gate_pre, up_pre, gate_taps, up_taps, down_proj, cotangent):
    row_count = gate_pre.shape[0]
    channels = gate_pre.shape[1]
    tap_count = gate_taps.shape[0]
    reach = tap_count - 1
    channel_start = lax.axis_index("tp") * channels
    gate_taps_f = lax.dynamic_slice_in_dim(gate_taps, channel_start, channels, 1).astype(
        jnp.float32
    )
    up_taps_f = lax.dynamic_slice_in_dim(up_taps, channel_start, channels, 1).astype(jnp.float32)
    before = from_behind((gate_pre[row_count - reach :], up_pre[row_count - reach :]), "fs", 1)
    gate_padded = jnp.concatenate([before[0], gate_pre], axis=0).astype(jnp.float32)
    up_padded = jnp.concatenate([before[1], up_pre], axis=0).astype(jnp.float32)
    gate_conv = gate_taps_f[0] * gate_padded[0:row_count]
    up_conv = up_taps_f[0] * up_padded[0:row_count]
    for offset in range(1, tap_count):
        gate_conv = gate_conv + gate_taps_f[offset] * gate_padded[offset : offset + row_count]
        up_conv = up_conv + up_taps_f[offset] * up_padded[offset : offset + row_count]
    gate_sigmoid = jax.nn.sigmoid(gate_conv)
    gate_act = gate_conv * gate_sigmoid
    hidden = (gate_act * up_conv).astype(jnp.bfloat16)
    whole_cot = lax.all_gather(cotangent, "tp", axis=0, tiled=True)
    cot_cols = whole_cot
    hidden_grad = lax.dot_general(
        cot_cols,
        lax.all_gather(down_proj, "fs", axis=1, tiled=True),
        (((1,), (1,)), ((), ())),
        preferred_element_type=jnp.float32,
    )
    gate_conv_grad = hidden_grad * up_conv * gate_sigmoid * (1.0 + gate_conv * (1.0 - gate_sigmoid))
    up_conv_grad = hidden_grad * gate_act
    following = from_behind((gate_conv_grad[0:reach], up_conv_grad[0:reach]), "fs", -1)
    gate_grad_pad = jnp.concatenate([gate_conv_grad, following[0]], axis=0)
    up_grad_pad = jnp.concatenate([up_conv_grad, following[1]], axis=0)
    gate_grad = gate_taps_f[0] * gate_grad_pad[reach : reach + row_count]
    up_grad = up_taps_f[0] * up_grad_pad[reach : reach + row_count]
    for offset in range(1, tap_count):
        lead = reach - offset
        gate_grad = gate_grad + gate_taps_f[offset] * gate_grad_pad[lead : lead + row_count]
        up_grad = up_grad + up_taps_f[offset] * up_grad_pad[lead : lead + row_count]
    gate_tap_terms = jnp.stack(
        [
            jnp.sum(gate_conv_grad * gate_padded[offset : offset + row_count], axis=0)
            for offset in range(tap_count)
        ]
    )
    up_tap_terms = jnp.stack(
        [
            jnp.sum(up_conv_grad * up_padded[offset : offset + row_count], axis=0)
            for offset in range(tap_count)
        ]
    )
    tap_terms = jnp.stack([gate_tap_terms, up_tap_terms])
    feature_count = whole_cot.shape[1]
    grad_scale = 1.0 / math.sqrt(row_count * lax.axis_size("fs"))
    cot_cols = whole_cot
    own_rows = (
        lax.psum_scatter(
            lax.dot_general(
                cot_cols, hidden, (((0,), (0,)), ((), ())), preferred_element_type=jnp.float32
            ),
            "fs",
            scatter_dimension=0,
            tiled=True,
        )
        * grad_scale
    )
    down_grad = own_rows.T
    partial_norms = jnp.sum(own_rows * own_rows, axis=0)
    norm_sum, tap_sum = lax.psum((partial_norms, tap_terms), "fs")
    row_norms = norm_sum / feature_count
    tap_grads = lax.all_gather(tap_sum * grad_scale, "tp", axis=2, tiled=True)
    return (
        gate_grad.astype(jnp.bfloat16),
        up_grad.astype(jnp.bfloat16),
        down_grad,
        row_norms,
        tap_grads,
    )


def solution(mesh):
    placed = (P("fs", "tp"), P("fs", "tp"), P(), P(), P("tp", "fs"), P(("fs", "tp"), None))
    return jax.shard_map(
        body,
        mesh=mesh,
        in_specs=placed,
        out_specs=(P("fs", "tp"), P("fs", "tp"), P("tp", "fs"), P("tp"), P()),
        check_vma=False,
    )
```

profile of v0, /device:TPU:0, one launch (start us, length us, event | category | flops | bytes accessed | tf_op | source)
XLA Modules:
  0.0 337.2 jit_solution(16197569232840858787)
XLA Ops:
  7.2 0.0 copy-start
  7.2 0.0 all-gather.3.cloned.1.call-start
  7.2 0.7 all-gather.3.cloned.1.call-update
  7.9 0.0 all-gather.5.cloned.1.call-start
  8.0 0.7 all-gather.5.cloned.1.call-update
  8.7 0.0 reduce-scatter.2.cloned.1.call-start
  8.7 0.7 slice.74
  9.5 2.4 collective-permute-start
  11.9 0.7 slice.80
  12.6 4.6 %collective-permute-start.1 = (bf16[2,1408]{1,0:T(2,128)(2,1)S(1)}, bf16[2,1408]{1,0:T(2,128)(2,1)S(1)}, u32[]{:S(2)}, u32[]{:S(2)}) collective-permute-start(bf16[2,1408]{1,0:T(2,128)(2,1)S(1)} %slice.80), channel_id=1, source_target_pairs={{0,4},{4,8},{8,12},{12,16},{16,20},{20,24},{24,28},{1,5},{5,9},{9,... | collective-permute-start | bytes 16904 | tf_op jit(solution)/shard_map/ppermute | solution.py:12
  17.2 0.7 dynamic-slice_convert_fusion
  18.0 0.1 slice_reduce_fusion.5
  18.0 0.0 collective-permute-done
  18.1 5.2 %maximum_convert_fusion = f32[1026,1408]{1,0:T(8,128)} fusion(bf16[1024,1408]{1,0:T(8,128)(2,1)} %param.7, bf16[2,1408]{1,0:T(2,128)(2,1)S(1)} %collective-permute-done), kind=kLoop, calls=%fused_computation.31 | loop fusion | flops 5778432 | bytes 8667648 | tf_op jit(solution)/shard_map/convert_element_type | solution.py:27
  23.2 0.0 collective-permute-done.1
  23.2 0.0 copy-done
  23.2 3.1 maximum_convert_fusion.1
  26.3 38.9 %all-gather.3.cloned.1.call-done = bf16[1024,2048]{1,0:T(8,128)(2,1)} async-done(((bf16[256,2048]{1,0:T(8,128)(2,1)}), bf16[1024,2048]{1,0:T(8,128)(2,1)}) %all-gather.3.cloned.1.call-update) | async-done | bytes 4194320 | tf_op jit(solution)/shard_map/all_gather | solution.py:36
  65.2 62.4 %all-gather.5.cloned.1.call-done = bf16[1408,2048]{1,0:T(8,128)(2,1)} async-done(((bf16[1408,256]{1,0:T(8,128)(2,1)}), bf16[1408,2048]{1,0:T(8,128)(2,1)}) %all-gather.5.cloned.1.call-update) | async-done | bytes 5767184 | tf_op jit(solution)/shard_map/all_gather | solution.py:40
  127.6 32.1 %multiply_reduce_fusion.5 = (f32[1408]{0:T(1024)S(1)}, f32[1408]{0:T(1024)S(1)}, f32[1408]{0:T(1024)S(1)}, f32[1024,1408]{1,0:T(8,128)}, f32[1024,1408]{1,0:T(8,...) fusion(f32[1026,1408]{1,0:T(8,128)} %maximum_convert_fusion.1, f32[1026,1408]{1,0:T(8,128)} %maximum_convert_fusion, ...), kind=kOutput, calls=%fused_computation.24 | convolution fusion | flops 5941620224 | bytes 67683840 | tf_op jit(solution)/shard_map/dot_general | solution.py:38
  159.7 14.2 %convolution_bitcast_fusion = f32[2048,1408]{0,1:T(8,128)} fusion(bf16[1024,2048]{1,0:T(8,128)(2,1)} %all-gather.3.cloned.1.call-done, f32[1024,1408]{1,0:T(8,128)} %get-tuple-element.25, f32[1024,1408]{1,0:T(8,128)} %get-tuple-element.26), kind=kOutput, calls=%fused_computation | convolution fusion | flops 5914230784 | bytes 27262976 | tf_op jit(solution)/shard_map/dot_general | solution.py:73
  173.8 0.0 slice-start
  173.8 0.0 reduce-scatter.2.cloned.1.call-update
  173.9 0.0 slice-start.1
  173.9 12.1 %multiply_reduce_fusion.2 = (f32[1408]{0:T(1024)S(1)}, f32[1408]{0:T(1024)S(1)}, f32[1408]{0:T(1024)S(1)}, f32[1024,1408]{1,0:T(8,128)S(1)}) fusion(f32[1026,1408]{1,0:T(8,128)} %maximum_convert_fusion, f32[1024,1408]{1,0:T(8,128)} %get-tuple-element.30, f32[1024,1408]{1,0:T(8,128)} %get-tuple-element.26), kind=kLoop, calls=%fused_computation.21 | loop fusion | flops 15855488 | bytes 34619904 | tf_op jit(solution)/shard_map/reduce_sum | solution.py:63
  186.1 0.0 slice-done
  186.1 0.0 slice-done.1
  186.2 1.3 collective-permute-start.2
  187.5 1.5 collective-permute-start.3
  189.0 0.2 collective-permute-done.2
  189.2 5.2 %fusion.9 = bf16[1024,1408]{1,0:T(8,128)(2,1)} fusion(f32[1024,1408]{1,0:T(8,128)S(1)} %bitcast.12, f32[2,1408]{1,0:T(2,128)S(1)} %collective-permute-done.2, f32[1408]{0:T(1024)S(1)} %get-tuple-element.20, f32[1408]{0:T(1024)S(1)} %get-tuple-element.21, f32[1408]{0:T(1024)S(1)} %get-tuple-element.19), kind=kLoop, calls=%fused_computation.14 | loop fusion | flops 11534336 | bytes 8678912 | tf_op jit(solution)/shard_map/convert_element_type | solution.py:88
  194.5 0.0 collective-permute-done.3
  194.5 5.3 %fusion.4 = bf16[1024,1408]{1,0:T(8,128)(2,1)} fusion(f32[1024,1408]{1,0:T(8,128)S(1)} %get-tuple-element.27, f32[2,1408]{1,0:T(2,128)S(1)} %collective-permute-done.3, f32[1408]{0:T(1024)S(1)} %get-tuple-element.17, f32[1408]{0:T(1024)S(1)} %get-tuple-element.18, f32[1408]{0:T(1024)S(1)} %get-tuple-element.16), kind=kLoop, calls=%fused_computation.9 | loop fusion | flops 11534336 | bytes 8678912 | tf_op jit(solution)/shard_map/convert_element_type | solution.py:89
  199.8 91.9 %reduce-scatter.2.cloned.1.call-done = f32[256,1408]{0,1:T(8,128)} async-done(((f32[2048,1408]{0,1:T(8,128)}), f32[256,1408]{0,1:T(8,128)}) %reduce-scatter.2.cloned.1.call-update) | async-done | bytes 1441808 | tf_op jit(solution)/shard_map/reduce_scatter | solution.py:72
  291.7 2.6 multiply_reduce_fusion.6
  294.3 26.4 %all-reduce = (f32[1408]{0:T(1024)S(1)}, f32[2,3,1408]{2,1,0:T(4,128)S(1)}) all-reduce(f32[1408]{0:T(1024)S(1)} %get-tuple-element.28, f32[2,3,1408]{2,1,0:T(4,128)S(1)} %pad_maximum_fusion.2), channel_id=1, replica_groups=mesh['fs'=8,'tp'=4] {'fs'}, use_global_device_ids=true, to_apply=%region_2.0 | all-reduce | flops 9856 | bytes 78848 | tf_op jit(solution)/shard_map/psum | solution.py:84
  320.6 0.6 broadcast_multiply_fusion.1
  321.2 8.7 %all_gather.11 = f32[2,3,5632]{2,1,0:T(4,128)S(1)} all-gather(f32[2,3,1408]{2,1,0:T(4,128)S(1)} %broadcast_multiply_fusion), channel_id=1, replica_groups=mesh['fs'=8,'tp'=4] {'tp'}, dimensions={2}, use_global_device_ids=true | all-gather | bytes 168960 | tf_op jit(solution)/shard_map/all_gather | solution.py:86
  329.9 0.7 copy.11
  (14 shorter events, 0.2 us)
Async XLA Ops:
  7.2 16.1 %copy-start = (bf16[1024,1408]{1,0:T(8,128)(2,1)S(1)}, bf16[1024,1408]{1,0:T(8,128)(2,1)}, u32[]{:S(2)}) copy-start(bf16[1024,1408]{1,0:T(8,128)(2,1)} %param.6) | copy-start | bytes 8650756
  7.2 58.0 %all-gather.3.cloned.1.call-start = ((), (), s32[]{:S(2)}) async-start(), calls=%async_computation.1 | async-start | bytes 5242880 | tf_op jit(solution)/shard_map/all_gather | solution.py:36
  7.9 119.7 %all-gather.5.cloned.1.call-start = ((), (), s32[]{:S(2)}) async-start(), calls=%async_computation.2 | async-start | bytes 6488064 | tf_op jit(solution)/shard_map/all_gather | solution.py:40
  8.7 283.0 %reduce-scatter.2.cloned.1.call-start = ((), (), s32[]{:S(2)}) async-start(), calls=%async_computation.3 | async-start | bytes 12976128 | tf_op jit(solution)/shard_map/reduce_scatter | solution.py:72
  9.5 8.6 %collective-permute-start = (bf16[2,1408]{1,0:T(2,128)(2,1)S(1)}, bf16[2,1408]{1,0:T(2,128)(2,1)S(1)}, u32[]{:S(2)}, u32[]{:S(2)}) collective-permute-start(bf16[2,1408]{1,0:T(2,128)(2,1)S(1)} %slice.74), channel_id=1, source_target_pairs={{0,4},{4,8},{8,12},{12,16},{16,20},{20,24},{24,28},{1,5},{5,9},{9,... | collective-permute-start | bytes 16904 | tf_op jit(solution)/shard_map/ppermute | solution.py:12
  12.6 10.6 %collective-permute-start.1 = (bf16[2,1408]{1,0:T(2,128)(2,1)S(1)}, bf16[2,1408]{1,0:T(2,128)(2,1)S(1)}, u32[]{:S(2)}, u32[]{:S(2)}) collective-permute-start(bf16[2,1408]{1,0:T(2,128)(2,1)S(1)} %slice.80), channel_id=1, source_target_pairs={{0,4},{4,8},{8,12},{12,16},{16,20},{20,24},{24,28},{1,5},{5,9},{9,... | collective-permute-start | bytes 16904 | tf_op jit(solution)/shard_map/ppermute | solution.py:12
  173.8 12.3 %slice-start = ((s8[5767168]{0:T(1024)(128)(4,1)}), s8[1572864]{0:T(1024)(128)(4,1)S(1)}, s32[]{:S(2)}) async-start(s8[5767168]{0:T(1024)(128)(4,1)} %bitcast.11), calls=%async_computation.4 | async-start | bytes 3145728
  173.9 12.3 %slice-start.1 = ((s8[5767168]{0:T(1024)(128)(4,1)}), s8[4194304]{0:T(1024)(128)(4,1)S(1)}, s32[]{:S(2)}) async-start(s8[5767168]{0:T(1024)(128)(4,1)} %bitcast.11), calls=%async_computation.5 | async-start | bytes 8388608
  186.2 3.1 collective-permute-start.2
  187.5 7.0 %collective-permute-start.3 = (f32[2,1408]{1,0:T(2,128)S(1)}, f32[2,1408]{1,0:T(2,128)S(1)}, u32[]{:S(2)}, u32[]{:S(2)}) collective-permute-start(f32[2,1408]{1,0:T(2,128)S(1)} %slice.107), channel_id=1, source_target_pairs={{4,0},{8,4},{12,8},{16,12},{20,16},{24,20},{28,24},{5,1},{9,5},{13... | collective-permute-start | bytes 33800 | tf_op jit(solution)/shard_map/ppermute | solution.py:12
Sparse Core Ops, SparseCore 0:
  9.8 55.2 all-gather.2
  66.7 60.7 all-gather.4
  174.0 117.6 reduce-scatter.1
where the time goes:
time: 338 us; the launch traced here: 337 us
  waiting for transfers between devices  195 us (58%)
  matrix products  46.2 us (14%)
  blocking collectives  35 us (10%)
  other arithmetic  34.9 us (10%)
  between operations  14 us (4%)
  starting transfers between devices  9.86 us (3%)
    reduce_scatter x1, waiting for transfers between devices, body(): lax.psum_scatter(lax.dot_general(cot_cols, hidden, (((0,), (0,)), ((), ()...  91.9 us
    all_gather x1, waiting for transfers between devices, body(): lax.all_gather(down_proj, 'fs', axis=1, tiled=True)  62.4 us
    all_gather x1, waiting for transfers between devices, body(): whole_cot = lax.all_gather(cotangent, 'tp', axis=0, tiled=True)  38.9 us
    dot_general x1, matrix products, body(): lax.dot_general(cot_cols, lax.all_gather(down_proj, 'fs', axis=1, tiled=T...  32.1 us
    psum x1, blocking collectives, body(): norm_sum, tap_sum = lax.psum((partial_norms, tap_terms), 'fs')  26.4 us
    dot_general x1, matrix products, body(): lax.dot_general(cot_cols, hidden, (((0,), (0,)), ((), ())), preferred_ele...  14.2 us
    reduce_sum x1, other arithmetic, body(): jnp.sum(up_conv_grad * up_padded[offset:offset + row_count], axis=0)  12.1 us
    ppermute x4, starting transfers between devices, from_behind(): return lax.ppermute(block, axis, route)  9.74 us
  transfers between devices with their start and end apart: 7, of which 4 were waited for; matrix products, arithmetic and copies ran while one was open for 10% of the time, Pallas kernels for 0%

commit v1 on v0

--- a/solution.py
+++ b/solution.py
@@ -1,9 +1,406 @@
+import functools
 import math
 
 import jax
 import jax.numpy as jnp
 from jax import lax
+from jax.experimental import pallas as pl
+from jax.experimental.pallas import tpu as pltpu
 from jax.sharding import PartitionSpec as P
+
+MESH = pl.DeviceIdType.MESH
+
+
+def snake(position, width):
+    row, column = position // width, position % width
+    return row * width + column + (row % 2) * (width - 1 - 2 * column)
+
+
+def conv_of(ref, halo_ref, taps_ref, start, count, columns):
+    reach = taps_ref.shape[0] - 1
+    here = ref[pl.ds(start, count), columns].astype(jnp.float32)
+    earlier = pl.multiple_of(jnp.maximum(start - 16, 0), 16)
+    tail = ref[pl.ds(earlier, 16), columns].astype(jnp.float32)[8:]
+    tail = jnp.where(start == 0, halo_ref[:, columns], tail)
+    rows = jnp.concatenate([tail, here], axis=0)
+    out = None
+    for offset in range(reach + 1):
+        lag = reach - offset
+        shifted = pltpu.roll(rows, lag, 0)[8:] if lag else here
+        term = taps_ref[offset : offset + 1, columns] * shifted
+        out = term if out is None else out + term
+    return out
+
+
+def gather_kernel(
+    chips,
+    tps,
+    cot_ref,
+    down_ref,
+    gate_ref,
+    up_ref,
+    gate_halo,
+    up_halo,
+    gate_taps,
+    up_taps,
+    cot_out,
+    down_out,
+    hidden_out,
+    *sems,
+):
+    (ring_send, ring_recv, line_send, line_recv, pair_send, pair_recv, local_sem) = sems
+    f, q = lax.axis_index("fs"), lax.axis_index("tp")
+    z, core = f // 2, f % 2
+    width = math.isqrt(tps)
+    spot = snake(q, width)
+    half_ring = tps // 2
+    ring_next = (snake((spot + 1) % tps, width), snake((spot + tps - 1) % tps, width))
+    rows = cot_ref.shape[0]
+    cols = down_ref.shape[1]
+    partner = z * 2 + 1 - core
+    behind, ahead = z > 0, z < chips - 1
+
+    barrier = pltpu.get_barrier_semaphore()
+    for device in ({"tp": ring_next[0]}, {"tp": ring_next[1]}, {"fs": partner}):
+        pl.semaphore_signal(barrier, inc=1, device_id=device, device_id_type=MESH)
+
+    @pl.when(behind)
+    def _():
+        pl.semaphore_signal(barrier, inc=1, device_id={"fs": f - 2}, device_id_type=MESH)
+
+    @pl.when(ahead)
+    def _():
+        pl.semaphore_signal(barrier, inc=1, device_id={"fs": f + 2}, device_id_type=MESH)
+
+    pl.semaphore_wait(barrier, 4 + (z + chips - 1) // chips - (z + 1) // chips)
+
+    def cot_rows(owner_spot, way, part):
+        owner = snake((owner_spot + 2 * tps) % tps, width)
+        if part:
+            return pl.ds(owner * rows + way * (rows // 2), rows // 2)
+        return pl.ds(owner * rows, rows)
+
+    def ring_copy(step, way):
+        sign = 1 - 2 * way
+        part = step == half_ring
+        where = cot_rows(spot - sign * (step - 1), way, part)
+        if step == 1:
+            src = cot_ref.at[pl.ds(way * (rows // 2), rows // 2)] if part else cot_ref
+        else:
+            src = cot_out.at[where]
+        return pltpu.make_async_remote_copy(
+            src_ref=src,
+            dst_ref=cot_out.at[where],
+            send_sem=ring_send.at[way, step - 1],
+            recv_sem=ring_recv.at[way, step - 1],
+            device_id={"tp": ring_next[way]},
+            device_id_type=MESH,
+        )
+
+    def ring_landing(step, way):
+        sign = 1 - 2 * way
+        where = cot_rows(spot - sign * step, way, step == half_ring)
+        return pltpu.make_async_remote_copy(
+            src_ref=cot_out.at[where],
+            dst_ref=cot_out.at[where],
+            send_sem=ring_send.at[way, step - 1],
+            recv_sem=ring_recv.at[way, step - 1],
+            device_id={"tp": ring_next[way]},
+            device_id_type=MESH,
+        )
+
+    def down_block(chip, which):
+        block = chip * 2 + which
+        if cols % 128:
+            return down_out.at[block]
+        return down_out.at[:, pl.ds(pl.multiple_of(block * cols, cols), cols)]
+
+    def line_copy(step, way):
+        sign = 1 - 2 * way
+        where = down_block(z - sign * (step - 1), core)
+        return pltpu.make_async_remote_copy(
+            src_ref=down_ref if step == 1 else where,
+            dst_ref=where,
+            send_sem=line_send.at[way, step - 1],
+            recv_sem=line_recv.at[way, step - 1],
+            device_id={"fs": f + 2 * sign},
+            device_id_type=MESH,
+        )
+
+    def line_landing(step, way):
+        sign = 1 - 2 * way
+        where = down_block(z - sign * step, core)
+        return pltpu.make_async_remote_copy(
+            src_ref=where,
+            dst_ref=where,
+            send_sem=line_send.at[way, step - 1],
+            recv_sem=line_recv.at[way, step - 1],
+            device_id={"fs": f + 2 * sign},
+            device_id_type=MESH,
+        )
+
+    def pair_copy(step, way, which):
+        sign = 1 - 2 * way
+        where = down_block(z - sign * step, which)
+        slot = step + way * (chips - 1)
+        return pltpu.make_async_remote_copy(
+            src_ref=down_ref if step == 0 else where,
+            dst_ref=where,
+            send_sem=pair_send.at[slot],
+            recv_sem=pair_recv.at[slot],
+            device_id={"fs": partner},
+            device_id_type=MESH,
+        )
+
+    def has_landing(step, way):
+        return z >= step if way == 0 else z + step < chips
+
+    def has_copy(step, way):
+        going = ahead if way == 0 else behind
+        return going if step == 1 else jnp.logical_and(going, has_landing(step - 1, way))
+
+    for way in range(2):
+        ring_copy(1, way).start()
+
+        @pl.when(has_copy(1, way))
+        def _():
+            line_copy(1, way).start()
+
+    pair_copy(0, 0, core).start()
+    own_cot = pltpu.make_async_copy(cot_ref, cot_out.at[pl.ds(q * rows, rows)], local_sem.at[0])
+    own_down = pltpu.make_async_copy(down_ref, down_block(z, core), local_sem.at[1])
+    own_cot.start()
+    own_down.start()
+
+    total_rows, channels = gate_ref.shape
+    count = math.gcd(total_rows, 64)
+
+    def hidden_rows(i, carry):
+        start = pl.multiple_of(i * count, count)
+        for left in range(0, channels, 128):
+            columns = pl.ds(left, min(128, channels - left))
+            gate_conv = conv_of(gate_ref, gate_halo, gate_taps, start, count, columns)
+            up_conv = conv_of(up_ref, up_halo, up_taps, start, count, columns)
+            hidden = gate_conv * jax.nn.sigmoid(gate_conv) * up_conv
+            hidden_out[pl.ds(start, count), columns] = hidden.astype(hidden_out.dtype)
+        return carry
+
+    lax.fori_loop(0, total_rows // count, hidden_rows, 0)
+
+    for step in range(1, max(chips - 1, half_ring) + 1):
+        if step <= chips - 1:
+            for way in range(2):
+
+                @pl.when(has_landing(step, way))
+                def _():
+                    line_landing(step, way).wait_recv()
+                    pair_copy(step, way, core).start()
+
+                if step + 1 <= chips - 1:
+
+                    @pl.when(has_copy(step + 1, way))
+                    def _():
+                        line_copy(step + 1, way).start()
+
+        if step <= half_ring:
+            for way in range(2):
+                ring_landing(step, way).wait_recv()
+                if step + 1 <= half_ring:
+                    ring_copy(step + 1, way).start()
+
+    own_cot.wait()
+    own_down.wait()
+    pair_copy(0, 0, 1 - core).wait_recv()
+    pair_copy(0, 0, core).wait_send()
+    for way in range(2):
+        for step in range(1, half_ring + 1):
+            ring_copy(step, way).wait_send()
+        for step in range(1, chips):
+
+            @pl.when(has_copy(step, way))
+            def _():
+                line_copy(step, way).wait_send()
+
+            @pl.when(has_landing(step, way))
+            def _():
+                pair_copy(step, way, 1 - core).wait_recv()
+                pair_copy(step, way, core).wait_send()
+
+
+def gather_both(cotangent, down_proj, *local):
+    fs, tps = lax.axis_size("fs"), lax.axis_size("tp")
+    chips = fs // 2
+    rows, features = cotangent.shape
+    channels, cols = down_proj.shape
+    dma = pltpu.SemaphoreType.DMA
+    down_shape = (fs, channels, cols) if cols % 128 else (channels, cols * fs)
+    whole_cot, whole_down, hidden = pl.pallas_call(
+        functools.partial(gather_kernel, chips, tps),
+        out_shape=(
+            jax.ShapeDtypeStruct((rows * tps, features), cotangent.dtype),
+            jax.ShapeDtypeStruct(down_shape, down_proj.dtype),
+            jax.ShapeDtypeStruct(local[0].shape, local[0].dtype),
+        ),
+        in_specs=[pl.BlockSpec(memory_space=pltpu.VMEM)] * (2 + len(local)),
+        out_specs=[
+            pl.BlockSpec(memory_space=pl.ANY),
+            pl.BlockSpec(memory_space=pl.ANY),
+            pl.BlockSpec(memory_space=pltpu.VMEM),
+        ],
+        scratch_shapes=[
+            dma((2, tps // 2)),
+            dma((2, tps // 2)),
+            dma((2, chips - 1)),
+            dma((2, chips - 1)),
+            dma((2 * chips - 1,)),
+            dma((2 * chips - 1,)),
+            dma((2,)),
+        ],
+        compiler_params=pltpu.CompilerParams(collective_id=0, has_side_effects=True),
+        name="gather_both",
+    )(cotangent, down_proj, *local)
+    if cols % 128:
+        whole_down = whole_down.transpose(1, 0, 2).reshape(channels, fs * cols)
+    return whole_cot, whole_down, hidden
+
+
+def small_kernel(fs, tps, mine_ref, sum_ref, all_ref, terms, total, sums, *sems):
+    send_a, recv_a, send_b, recv_b = sems
+    f, q = lax.axis_index("fs"), lax.axis_index("tp")
+    barrier = pltpu.get_barrier_semaphore()
+    for i in range(1, fs):
+        pl.semaphore_signal(
+            barrier, inc=1, device_id={"fs": (f + i) % fs}, device_id_type=MESH
+        )
+    for i in range(1, tps):
+        pl.semaphore_signal(
+            barrier, inc=1, device_id={"tp": (q + i) % tps}, device_id_type=MESH
+        )
+    pl.semaphore_wait(barrier, fs + tps - 2)
+
+    def over_fs(i):
+        return pltpu.make_async_remote_copy(
+            src_ref=mine_ref,
+            dst_ref=terms.at[f],
+            send_sem=send_a.at[i],
+            recv_sem=recv_a.at[i],
+            device_id={"fs": (f + i) % fs},
+            device_id_type=MESH,
+        )
+
+    def over_tp(i):
+        return pltpu.make_async_remote_copy(
+            src_ref=total,
+            dst_ref=sums.at[q],
+            send_sem=send_b.at[i],
+            recv_sem=recv_b.at[i],
+            device_id={"tp": (q + i) % tps},
+            device_id_type=MESH,
+        )
+
+    def landing(buffer, slot, send, recv, i, device):
+        return pltpu.make_async_remote_copy(
+            src_ref=buffer.at[slot],
+            dst_ref=buffer.at[slot],
+            send_sem=send.at[i],
+            recv_sem=recv.at[i],
+            device_id=device,
+            device_id_type=MESH,
+        )
+
+    for i in range(1, fs):
+        over_fs(i).start()
+    terms[f] = mine_ref[...]
+    for i in range(1, fs):
+        landing(terms, (f + fs - i) % fs, send_a, recv_a, i, {"fs": (f + i) % fs}).wait_recv()
+    added = terms[0]
+    for i in range(1, fs):
+        added = added + terms[i]
+    total[...] = added
+    sum_ref[...] = added
+    sums[q] = added
+    for i in range(1, fs):
+        over_fs(i).wait_send()
+    for i in range(1, tps):
+        over_tp(i).start()
+    for i in range(1, tps):
+        landing(sums, (q + tps - i) % tps, send_b, recv_b, i, {"tp": (q + i) % tps}).wait_recv()
+    all_ref[...] = sums[...]
+    for i in range(1, tps):
+        over_tp(i).wait_send()
+
+
+def small_sums(mine, identity):
+    fs, tps = lax.axis_size("fs"), lax.axis_size("tp")
+    dma = pltpu.SemaphoreType.DMA
+    shape = mine.shape
+    return pl.pallas_call(
+        functools.partial(small_kernel, fs, tps),
+        out_shape=(
+            jax.ShapeDtypeStruct(shape, jnp.float32),
+            jax.ShapeDtypeStruct((tps,) + shape, jnp.float32),
+        ),
+        in_specs=[pl.BlockSpec(memory_space=pltpu.VMEM)],
+        out_specs=[pl.BlockSpec(memory_space=pltpu.VMEM)] * 2,
+        scratch_shapes=[
+            pltpu.VMEM((fs,) + shape, jnp.float32),
+            pltpu.VMEM(shape, jnp.float32),
+            pltpu.VMEM((tps,) + shape, jnp.float32),
+            dma((fs,)),
+            dma((fs,)),
+            dma((tps,)),
+            dma((tps,)),
+        ],
+        compiler_params=pltpu.CompilerParams(collective_id=identity, has_side_effects=True),
+        name=f"small_sums_{identity}",
+    )(mine)
+
+
+def norm_kernel(fs, mine_ref, sum_ref, terms, send, recv):
+    f = lax.axis_index("fs")
+    barrier = pltpu.get_barrier_semaphore()
+    for i in range(1, fs):
+        pl.semaphore_signal(
+            barrier, inc=1, device_id={"fs": (f + i) % fs}, device_id_type=MESH
+        )
+    pl.semaphore_wait(barrier, fs - 1)
+
+    def copy(i, src, slot):
+        return pltpu.make_async_remote_copy(
+            src_ref=src,
+            dst_ref=terms.at[slot],
+            send_sem=send.at[i],
+            recv_sem=recv.at[i],
+            device_id={"fs": (f + i) % fs},
+            device_id_type=MESH,
+        )
+
+    for i in range(1, fs):
+        copy(i, mine_ref, f).start()
+    terms[f] = mine_ref[...]
+    for i in range(1, fs):
+        slot = (f + fs - i) % fs
+        copy(i, terms.at[slot], slot).wait_recv()
+    added = terms[0]
+    for i in range(1, fs):
+        added = added + terms[i]
+    sum_ref[...] = added
+    for i in range(1, fs):
+        copy(i, mine_ref, f).wait_send()
+
+
+def norm_sum(mine, identity):
+    fs = lax.axis_size("fs")
+    dma = pltpu.SemaphoreType.DMA
+    return pl.pallas_call(
+        functools.partial(norm_kernel, fs),
+        out_shape=jax.ShapeDtypeStruct(mine.shape, jnp.float32),
+        in_specs=[pl.BlockSpec(memory_space=pltpu.VMEM)],
+        out_specs=pl.BlockSpec(memory_space=pltpu.VMEM),
+        scratch_shapes=[pltpu.VMEM((fs,) + mine.shape, jnp.float32), dma((fs,)), dma((fs,))],
+        compiler_params=pltpu.CompilerParams(collective_id=identity, has_side_effects=True),
+        name="norm_sum",
+    )(mine)
 
 
 def from_behind(block, axis, distance):
@@ -23,6 +420,35 @@
     )
     up_taps_f = lax.dynamic_slice_in_dim(up_taps, channel_start, channels, 1).astype(jnp.float32)
     before = from_behind((gate_pre[row_count - reach :], up_pre[row_count - reach :]), "fs", 1)
+    halo = [
+        jnp.concatenate([jnp.zeros((8 - reach, channels), jnp.float32), part.astype(jnp.float32)])
+        for part in before
+    ]
+    whole_cot, whole_down, hidden = gather_both(
+        cotangent, down_proj, gate_pre, up_pre, halo[0], halo[1], gate_taps_f, up_taps_f
+    )
+    grad_scale = 1.0 / math.sqrt(row_count * lax.axis_size("fs"))
+    fs = lax.axis_size("fs")
+    sum_type = jnp.bfloat16 if fs <= 8 else jnp.float32
+    core = lax.axis_index("fs") % 2
+    every_term = lax.dot_general(
+        whole_cot, hidden, (((0,), (0,)), ((), ())), preferred_element_type=jnp.float32
+    ).reshape(fs // 2, 2, -1, channels)
+
+    def terms_of(which):
+        return lax.dynamic_index_in_dim(every_term, which, 1, keepdims=False).reshape(-1, channels)
+
+    given = terms_of(1 - core).astype(sum_type)
+    taken = lax.ppermute(given, "fs", [(i, i ^ 1) for i in range(fs)])
+    terms = (terms_of(core) + taken.astype(jnp.float32)).astype(sum_type)
+    terms, whole_down, gate_pre, up_pre, before = lax.optimization_barrier(
+        (terms, whole_down, gate_pre, up_pre, before)
+    )
+    groups = [list(range(which, fs, 2)) for which in range(2)]
+    own_rows = lax.psum_scatter(
+        terms, "fs", scatter_dimension=0, tiled=True, axis_index_groups=groups
+    )
+    own_rows = own_rows.astype(jnp.float32) * grad_scale
     gate_padded = jnp.concatenate([before[0], gate_pre], axis=0).astype(jnp.float32)
     up_padded = jnp.concatenate([before[1], up_pre], axis=0).astype(jnp.float32)
     gate_conv = gate_taps_f[0] * gate_padded[0:row_count]
@@ -32,12 +458,9 @@
         up_conv = up_conv + up_taps_f[offset] * up_padded[offset : offset + row_count]
     gate_sigmoid = jax.nn.sigmoid(gate_conv)
     gate_act = gate_conv * gate_sigmoid
-    hidden = (gate_act * up_conv).astype(jnp.bfloat16)
-    whole_cot = lax.all_gather(cotangent, "tp", axis=0, tiled=True)
-    cot_cols = whole_cot
     hidden_grad = lax.dot_general(
-        cot_cols,
-        lax.all_gather(down_proj, "fs", axis=1, tiled=True),
+        whole_cot,
+        whole_down,
         (((1,), (1,)), ((), ())),
         preferred_element_type=jnp.float32,
     )
@@ -66,24 +489,15 @@
     )
     tap_terms = jnp.stack([gate_tap_terms, up_tap_terms])
     feature_count = whole_cot.shape[1]
-    grad_scale = 1.0 / math.sqrt(row_count * lax.axis_size("fs"))
-    cot_cols = whole_cot
-    own_rows = (
-        lax.psum_scatter(
-            lax.dot_general(
-                cot_cols, hidden, (((0,), (0,)), ((), ())), preferred_element_type=jnp.float32
-            ),
-            "fs",
-            scatter_dimension=0,
-            tiled=True,
-        )
-        * grad_scale
-    )
     down_grad = own_rows.T
     partial_norms = jnp.sum(own_rows * own_rows, axis=0)
-    norm_sum, tap_sum = lax.psum((partial_norms, tap_terms), "fs")
-    row_norms = norm_sum / feature_count
-    tap_grads = lax.all_gather(tap_sum * grad_scale, "tp", axis=2, tiled=True)
+    tap_rows = tap_terms.reshape(2 * tap_count, channels)
+    spare = jnp.zeros((-(2 * tap_count) % 8, channels), jnp.float32)
+    _, everywhere = small_sums(jnp.concatenate([tap_rows, spare], axis=0), 1)
+    row_norms = norm_sum(partial_norms[None], 2)[0] / feature_count
+    tap_grads = (
+        everywhere[:, : 2 * tap_count].transpose(1, 0, 2).reshape(2, tap_count, -1) * grad_scale
+    )
     return (
         gate_grad.astype(jnp.bfloat16),
         up_grad.astype(jnp.bfloat16),

time: 338 us -> 225 us (0.67)
  waiting for transfers between devices: 195 us -> 0.03 us
  Pallas kernels: 0 us -> 86.2 us
  blocking collectives: 35 us -> 0 us
  local copies, waits for them, and re-layouts: 2.38 us -> 24.5 us
  other arithmetic: 34.9 us -> 49.7 us
  matrix products: 46.2 us -> 39.3 us
    all_gather x2 -> x0, waiting for transfers between devices: 101 us -> none  [the longest x1 62.4 us: body(): lax.all_gather(down_proj, 'fs', axis=1, tiled=True)]
    reduce_scatter x1, waiting for transfers between devices: 91.9 us -> 0.01 us  [body(): lax.psum_scatter(terms, 'fs', scatter_dimension=0, tiled=True, axis_index...]
    pallas_call x0 -> x3, Pallas kernels: none -> 86.2 us  [the longest x1 59.3 us: gather_both(): pl.pallas_call(functools.partial(gather_kernel, chips, tps), out_shape=(j...]
    psum x1 -> x0, blocking collectives: 26.4 us -> none  [body(): norm_sum, tap_sum = lax.psum((partial_norms, tap_terms), 'fs')]
    all_gather x1 -> x0, blocking collectives: 8.68 us -> none  [body(): tap_grads = lax.all_gather(tap_sum * grad_scale, 'tp', axis=2, tiled=True)]
    dot_general x2, matrix products: 46.2 us -> 39.3 us  [the longest x1 29.8 us: body(): lax.dot_general(whole_cot, whole_down, (((1,), (1,)), ((), ())), preferre...]
    reshape x0 -> x2, local copies, waits for them, and re-layouts: none -> 6.32 us  [the longest x1 6.3 us: terms_of(): lax.dynamic_index_in_dim(every_term, which, 1, keepdims=False)]
    convert_element_type x0 -> x1, other arithmetic: none -> 6.32 us  [body(): terms = (terms_of(core) + taken.astype(jnp.float32)).astype(sum_type)]
  transfers between devices with their start and end apart: 7 -> 6, of which waited for: 4 -> 0; matrix products, arithmetic and copies ran while one was open for 10% -> 38% of each run, Pallas kernels for 0% -> 8%
where the time goes in v1:
time: 225 us; the launch traced here: 224 us
  Pallas kernels  86.2 us (38%)
  other arithmetic  49.7 us (22%)
  matrix products  39.3 us (17%)
  local copies, waits for them, and re-layouts  24.5 us (11%)
  between operations  14.3 us (6%)
  starting transfers between devices  9.96 us (4%)
    pallas_call x1, Pallas kernels, gather_both(): pl.pallas_call(functools.partial(gather_kernel, chips, tps), out_shape=(j...  59.3 us
    dot_general x1, matrix products, body(): lax.dot_general(whole_cot, whole_down, (((1,), (1,)), ((), ())), preferre...  29.8 us
    pallas_call x1, Pallas kernels, small_sums(): pl.pallas_call(functools.partial(small_kernel, fs, tps), out_shape=(jax.S...  19 us
    reduce_sum x1, other arithmetic, body(): jnp.sum(up_conv_grad * up_padded[offset:offset + row_count], axis=0)  13.7 us
    convert_element_type x1, other arithmetic, body(): gate_grad.astype(jnp.bfloat16)  11.1 us
    ppermute x4, starting transfers between devices, from_behind(): return lax.ppermute(block, axis, route)  9.55 us
    dot_general x1, matrix products, body(): lax.dot_general(whole_cot, hidden, (((0,), (0,)), ((), ())), preferred_el...  9.53 us
    pallas_call x1, Pallas kernels, norm_sum(): pl.pallas_call(functools.partial(norm_kernel, fs), out_shape=jax.ShapeDty...  7.91 us
  transfers between devices with their start and end apart: 6, of which 0 were waited for; matrix products, arithmetic and copies ran while one was open for 38% of the time, Pallas kernels for 8%

profile of v1, /device:TPU:0, one launch (start us, length us, event | category | flops | bytes accessed | tf_op | source)
XLA Modules:
  0.0 224.0 jit_solution(9271606614219892520)
XLA Ops:
  7.2 0.0 reduce-scatter.2.cloned.1.call-start
  7.2 0.7 slice.77
  8.0 2.4 %collective-permute-start.1 = (bf16[2,1408]{1,0:T(2,128)(2,1)S(1)}, bf16[2,1408]{1,0:T(2,128)(2,1)S(1)}, u32[]{:S(2)}, u32[]{:S(2)}) collective-permute-start(bf16[2,1408]{1,0:T(2,128)(2,1)S(1)} %slice.77), channel_id=1, source_target_pairs={{0,4},{4,8},{8,12},{12,16},{16,20},{20,24},{24,28},{1,5},{5,9},{9,... | collective-permute-start | bytes 16904 | tf_op jit(solution)/shard_map/ppermute | solution.py:409
  10.4 0.7 slice.76
  11.1 4.6 %collective-permute-start = (bf16[2,1408]{1,0:T(2,128)(2,1)S(1)}, bf16[2,1408]{1,0:T(2,128)(2,1)S(1)}, u32[]{:S(2)}, u32[]{:S(2)}) collective-permute-start(bf16[2,1408]{1,0:T(2,128)(2,1)S(1)} %slice.76), channel_id=1, source_target_pairs={{0,4},{4,8},{8,12},{12,16},{16,20},{20,24},{24,28},{1,5},{5,9},{9,... | collective-permute-start | bytes 16904 | tf_op jit(solution)/shard_map/ppermute | solution.py:409
  15.7 1.3 dynamic-slice_convert_fusion.1
  17.0 0.0 collective-permute-done
  17.0 0.6 pad_convert_fusion.1.gate_halo
  17.7 0.0 collective-permute-done.1
  17.7 0.6 pad_convert_fusion.up_halo
  18.3 59.3 %gather_both.1 = (bf16[1024,2048]{1,0:T(8,128)(2,1)}, bf16[1408,2048]{1,0:T(8,128)(2,1)}, bf16[1024,1408]{1,0:T(8,128)(2,1)}) custom-call(bf16[256,2048]{1,0:T(8,128)(2,1)} %cot_ref.1, bf16[1408,256]{1,0:T(8,128)(2,1)} %down_ref.1, bf16[1024,1408]{1,0:T(8,128)(2,1)} %gate_ref.1, bf16[1024,1408]{1,0:T(8,128)(2,1)} %up_ref.1, ...), custom_call_target="tpu_custom_call" | custom-call | tf_op jit(solution)/shard_map/gather_both/pallas_call | solution.py:237
  77.6 9.5 %fusion.13 = f32[2048,1408]{1,0:T(8,128)S(1)} fusion(bf16[1024,2048]{1,0:T(8,128)(2,1)} %get-tuple-element.15, bf16[1024,1408]{1,0:T(8,128)(2,1)} %get-tuple-element.16), kind=kOutput, calls=%fused_computation.51 | convolution fusion | flops 5905580032 | bytes 18612224 | tf_op jit(solution)/shard_map/dot_general | solution.py:434
  87.2 0.0 copy-start.2
  87.2 4.3 %copy-done.2 = f32[2048,1408]{1,0:T(8,128)} copy-done((f32[2048,1408]{1,0:T(8,128)}, f32[2048,1408]{1,0:T(8,128)S(1)}, u32[]{:S(2)}) %copy-start.2) | copy-done | bytes 11534360
  91.5 0.3 dynamic-slice_convert_fusion
  91.8 2.7 %copy.18 = bf16[1024,1408]{0,1:T(8,128)(2,1)} copy(bf16[1024,1408]{1,0:T(8,128)(2,1)S(1)} %bitcast.18) | data formatting | bytes 5767168 | tf_op jit(solution)/shard_map/convert_element_type | solution.py:441
  94.5 0.4 collective-permute-start.2
  94.9 0.0 copy-done.4
  95.0 0.0 copy-done.3
  95.0 0.1 slice_reduce_fusion.5
  95.0 5.5 %constant_dynamic-slice_fusion = f32[4,1,256,1408]{3,2,1,0:T(8,128)} fusion(f32[4,2,256,1408]{3,2,1,0:T(8,128)} %bitcast.20, s32[]{:T(128)S(6)} %select_n.20), kind=kLoop, calls=%fused_computation.50 | loop fusion | bytes 11534340 | tf_op jit(solution)/shard_map/jit(dynamic_index_in_dim)/dynamic_slice | solution.py:439
  100.5 6.3 %copy.17 = f32[1024,1408]{0,1:T(8,128)} copy(f32[1024,1408]{1,0:T(8,128)} %bitcast.17) | data formatting | bytes 11534336 | tf_op jit(solution)/shard_map/reshape | solution.py:439
  106.8 0.0 collective-permute-done.2
  106.8 6.3 %add_convert_fusion = bf16[1024,1408]{0,1:T(8,128)(2,1)} fusion(f32[1024,1408]{0,1:T(8,128)} %copy.17, bf16[1024,1408]{0,1:T(8,128)(2,1)} %collective-permute-done.2), kind=kLoop, calls=%fused_computation.28 | loop fusion | flops 4325376 | bytes 11534336 | tf_op jit(solution)/shard_map/convert_element_type | solution.py:443
  113.1 0.0 reduce-scatter.2.cloned.1.call-update
  113.1 0.0 copy-done
  113.2 0.0 copy-start.1
  113.2 3.0 %maximum_convert_fusion = f32[1026,1408]{1,0:T(8,128)} fusion(bf16[1024,1408]{1,0:T(8,128)(2,1)S(1)} %copy-done, bf16[2,1408]{1,0:T(2,128)(2,1)S(1)} %collective-permute-done.1), kind=kLoop, calls=%fused_computation.30 | loop fusion | flops 5778432 | bytes 8667648 | tf_op jit(solution)/shard_map/convert_element_type | solution.py:453
  116.2 3.0 %maximum_convert_fusion.1 = f32[1026,1408]{1,0:T(8,128)} fusion(bf16[1024,1408]{1,0:T(8,128)(2,1)S(1)} %copy-done.1, bf16[2,1408]{1,0:T(2,128)(2,1)S(1)} %collective-permute-done), kind=kLoop, calls=%fused_computation.31 | loop fusion | flops 5778432 | bytes 8667648 | tf_op jit(solution)/shard_map/convert_element_type | solution.py:452
  119.2 29.8 %multiply_reduce_fusion.5 = (f32[1408]{0:T(1024)S(1)}, f32[1408]{0:T(1024)S(1)}, f32[1408]{0:T(1024)S(1)}, f32[1024,1408]{1,0:T(8,128)}, f32[1024,1408]{1,0:T(8,128)}, /*index=5*/f32[1024,1408]{1,0:T(8,128)}) fusion(f32[1026,1408]{1,0:T(8,128)} %maximum_convert_fusion.1, f32[1026,1408]{1,0:T(8,128)} %maximum_convert_fusion, ...), kind=kOutput, calls=%fused_computation.23 | convolution fusion | flops 5941620224 | bytes 61916672 | tf_op jit(solution)/shard_map/dot_general | solution.py:461
  149.0 13.7 %multiply_reduce_fusion.2 = (f32[1408]{0:T(1024)S(1)}, f32[1408]{0:T(1024)S(1)}, f32[1408]{0:T(1024)S(1)}, f32[1024,1408]{1,0:T(8,128)}) fusion(f32[1026,1408]{1,0:T(8,128)} %maximum_convert_fusion, f32[1024,1408]{1,0:T(8,128)} %get-tuple-element.47, f32[1024,1408]{1,0:T(8,128)} %get-tuple-element.43), kind=kLoop, calls=%fused_computation.20 | loop fusion | flops 15855488 | bytes 34619904 | tf_op jit(solution)/shard_map/reduce_sum | solution.py:486
  162.9 0.9 slice.111
  163.8 0.8 slice.108
  164.6 1.3 collective-permute-start.3
  165.9 1.3 collective-permute-start.4
  167.2 0.6 concatenate.33.mine_ref
  167.8 19.0 %small_sums_1.1 = (f32[8,1408]{1,0:T(8,128)}, f32[4,8,1408]{2,1,0:T(8,128)}) custom-call(f32[8,1408]{1,0:T(8,128)} %concatenate.33.mine_ref), custom_call_target="tpu_custom_call" | custom-call | tf_op jit(solution)/shard_map/small_sums_1/pallas_call | solution.py:337
  186.8 0.9 multiply_bitcast_fusion
  187.8 0.1 mul.199
  187.8 0.7 copy.16
  188.6 0.0 collective-permute-done.3
  188.6 11.1 %fusion.9 = bf16[1024,1408]{1,0:T(8,128)(2,1)} fusion(f32[1024,1408]{1,0:T(8,128)} %get-tuple-element.42, f32[2,1408]{1,0:T(2,128)S(1)} %collective-permute-done.3, f32[1408]{0:T(1024)S(1)} %get-tuple-element.40, f32[1408]{0:T(1024)S(1)} %get-tuple-element.41, f32[1408]{0:T(1024)S(1)} %get-tuple-element.39), kind=kLoop, calls=%fused_computation.13 | loop fusion | flops 11534336 | bytes 8678912 | tf_op jit(solution)/shard_map/convert_element_type | solution.py:502
  199.7 0.0 collective-permute-done.4
  199.7 5.2 %fusion.4 = bf16[1024,1408]{1,0:T(8,128)(2,1)} fusion(f32[1024,1408]{1,0:T(8,128)S(1)} %bitcast.16, f32[2,1408]{1,0:T(2,128)S(1)} %collective-permute-done.4, f32[1408]{0:T(1024)S(1)} %get-tuple-element.37, f32[1408]{0:T(1024)S(1)} %get-tuple-element.38, f32[1408]{0:T(1024)S(1)} %get-tuple-element.36), kind=kLoop, calls=%fused_computation.8 | loop fusion | flops 11534336 | bytes 8678912 | tf_op jit(solution)/shard_map/convert_element_type | solution.py:503
  205.0 2.4 %multiply_reduce_fusion.6 = (f32[1408]{0:T(1024)S(1)}, f32[1408,256]{1,0:T(8,128)}) fusion(bf16[256,1408]{0,1:T(8,128)(2,1)} %reduce-scatter.2.cloned.1.call-done), kind=kLoop, calls=%fused_computation.32 | loop fusion | flops 1440384 | bytes 2168320 | tf_op jit(solution)/shard_map/reduce_sum | solution.py:493
  207.4 0.6 broadcast_in_dim.4.mine_ref
  208.0 7.9 %norm_sum.1 = f32[1,1408]{1,0:T(1,128)} custom-call(f32[1,1408]{1,0:T(1,128)} %broadcast_in_dim.4.mine_ref), custom_call_target="tpu_custom_call" | custom-call | tf_op jit(solution)/shard_map/norm_sum/pallas_call | solution.py:395
  215.9 1.3 multiply_reduce_fusion.7
  (22 shorter events, 0.2 us)
Async XLA Ops:
  7.2 197.8 %reduce-scatter.2.cloned.1.call-start = ((), (), s32[]{:S(2)}) async-start(), calls=%async_computation.1 | async-start | bytes 3604480 | tf_op jit(solution)/shard_map/reduce_scatter | solution.py:448
  8.0 9.7 %collective-permute-start.1 = (bf16[2,1408]{1,0:T(2,128)(2,1)S(1)}, bf16[2,1408]{1,0:T(2,128)(2,1)S(1)}, u32[]{:S(2)}, u32[]{:S(2)}) collective-permute-start(bf16[2,1408]{1,0:T(2,128)(2,1)S(1)} %slice.77), channel_id=1, source_target_pairs={{0,4},{4,8},{8,12},{12,16},{16,20},{20,24},{24,28},{1,5},{5,9},{9,... | collective-permute-start | bytes 16904 | tf_op jit(solution)/shard_map/ppermute | solution.py:409
  11.1 5.9 %collective-permute-start = (bf16[2,1408]{1,0:T(2,128)(2,1)S(1)}, bf16[2,1408]{1,0:T(2,128)(2,1)S(1)}, u32[]{:S(2)}, u32[]{:S(2)}) collective-permute-start(bf16[2,1408]{1,0:T(2,128)(2,1)S(1)} %slice.76), channel_id=1, source_target_pairs={{0,4},{4,8},{8,12},{12,16},{16,20},{20,24},{24,28},{1,5},{5,9},{9,... | collective-permute-start | bytes 16904 | tf_op jit(solution)/shard_map/ppermute | solution.py:409
  87.2 4.3 %copy-start.2 = (f32[2048,1408]{1,0:T(8,128)}, f32[2048,1408]{1,0:T(8,128)S(1)}, u32[]{:S(2)}) copy-start(f32[2048,1408]{1,0:T(8,128)S(1)} %fusion.13) | copy-start | bytes 34603012
  91.5 3.4 %copy-start.4 = (f32[3,1408]{1,0:T(4,128)S(1)}, f32[3,1408]{1,0:T(4,128)}, u32[]{:S(2)}) copy-start(f32[3,1408]{1,0:T(4,128)} %get-tuple-element.48.up_taps) | copy-start | bytes 50692
  91.5 3.5 %copy-start.3 = (f32[3,1408]{1,0:T(4,128)S(1)}, f32[3,1408]{1,0:T(4,128)}, u32[]{:S(2)}) copy-start(f32[3,1408]{1,0:T(4,128)} %get-tuple-element.49.gate_taps) | copy-start | bytes 50692
  94.5 12.3 %collective-permute-start.2 = (bf16[1024,1408]{0,1:T(8,128)(2,1)}, bf16[1024,1408]{0,1:T(8,128)(2,1)}, u32[]{:S(2)}, u32[]{:S(2)}) collective-permute-start(bf16[1024,1408]{0,1:T(8,128)(2,1)} %copy.18), channel_id=1, source_target_pairs={{0,4},{4,0},{8,12},{12,8},{16,20},{20,16},{24,28},{28,24},{1,5},{5... | collective-permute-start | bytes 8650760 | tf_op jit(solution)/shard_map/ppermute | solution.py:442
  106.8 6.3 %copy-start = (bf16[1024,1408]{1,0:T(8,128)(2,1)S(1)}, bf16[1024,1408]{1,0:T(8,128)(2,1)}, u32[]{:S(2)}) copy-start(bf16[1024,1408]{1,0:T(8,128)(2,1)} %up_ref.1) | copy-start | bytes 8650756
  113.2 3.0 %copy-start.1 = (bf16[1024,1408]{1,0:T(8,128)(2,1)S(1)}, bf16[1024,1408]{1,0:T(8,128)(2,1)}, u32[]{:S(2)}) copy-start(bf16[1024,1408]{1,0:T(8,128)(2,1)} %gate_ref.1) | copy-start | bytes 8650756
  162.7 37.0 %slice-start = ((s8[5767168]{0:T(1024)(128)(4,1)}), s8[1572864]{0:T(1024)(128)(4,1)S(1)}, s32[]{:S(2)}) async-start(s8[5767168]{0:T(1024)(128)(4,1)} %bitcast.15), calls=%async_computation.2 | async-start | bytes 3145728
  164.6 24.0 %collective-permute-start.3 = (f32[2,1408]{1,0:T(2,128)S(1)}, f32[2,1408]{1,0:T(2,128)S(1)}, u32[]{:S(2)}, u32[]{:S(2)}) collective-permute-start(f32[2,1408]{1,0:T(2,128)S(1)} %slice.108), channel_id=1, source_target_pairs={{4,0},{8,4},{12,8},{16,12},{20,16},{24,20},{28,24},{5,1},{9,5},{13... | collective-permute-start | bytes 33800 | tf_op jit(solution)/shard_map/ppermute | solution.py:409
  165.9 33.9 %collective-permute-start.4 = (f32[2,1408]{1,0:T(2,128)S(1)}, f32[2,1408]{1,0:T(2,128)S(1)}, u32[]{:S(2)}, u32[]{:S(2)}) collective-permute-start(f32[2,1408]{1,0:T(2,128)S(1)} %slice.111), channel_id=1, source_target_pairs={{4,0},{8,4},{12,8},{16,12},{20,16},{24,20},{28,24},{5,1},{9,5},{13... | collective-permute-start | bytes 33800 | tf_op jit(solution)/shard_map/ppermute | solution.py:409
  188.6 11.2 %slice-start.1 = ((s8[5767168]{0:T(1024)(128)(4,1)}), s8[4194304]{0:T(1024)(128)(4,1)S(1)}, s32[]{:S(2)}) async-start(s8[5767168]{0:T(1024)(128)(4,1)} %bitcast.15), calls=%async_computation.3 | async-start | bytes 8388608
Sparse Core Ops, SparseCore 0:
  113.3 55.6 reduce-scatter.1
